TPU v7x, 512 devices: a 8x2x16 block of a 8x16x16 slice. The times are simulated.
512 devices in a mesh: grp: 2 (over y), fs: 16 (over z), tp: 16 (over x, core).
Axes of the slice: x: 8, y: 2, z: 16, core: 2. Of those that a mesh axis runs over, the one named last changes fastest.
The devices are a block of a 8x16x16 slice.
Arguments:
- tokens: bfloat16 [8192, 2048], P(('grp', 'fs'), 'tp'), parts along dimension 0, may hold values from -6 to 6
- route_experts: int32 [8192, 2], P(('grp', 'fs')), parts along dimension 0, may hold values from 0 to 15, as said below
- group_weight: float32 [8192], P(('grp', 'fs')), parts along dimension 0, may hold values from 0.2 to 1
- pair_logit: float32 [8192], P(('grp', 'fs')), parts along dimension 0, may hold values from -6 to 6
- norm_gain: float32 [2048], replicated, may hold values from 0.1 to 1.9
- gate_train: float32 [16, 2048, 2048], P(None, 'fs', 'tp'), may hold values from -0.125 to 0.125
- up_train: float32 [16, 2048, 2048], P(None, 'fs', 'tp'), may hold values from -0.125 to 0.125
- down_train: float32 [16, 2048, 2048], P(None, 'fs', 'tp'), may hold values from -0.125 to 0.125
Outputs:
- gate_serve: bfloat16 [32, 2048, 2048], P(('grp', 'fs'), None, 'tp'), parts along dimension 0
- up_serve: bfloat16 [32, 2048, 2048], P(('grp', 'fs'), None, 'tp'), parts along dimension 0
- down_serve: bfloat16 [32, 2048, 2048], P(('grp', 'fs'), None, 'tp'), parts along dimension 0
- moe_out: bfloat16 [8192, 2048], P(('grp', 'fs'), 'tp'), parts along dimension 0
There are 2 independent parts, one for each index of `grp`. A program takes and returns all parts, laid end to end along the dimension named above; an argument that names none is the same for every part. Nothing has to cross between parts.
Inputs may be any that keep to these rules, and one draw needn't show every extreme that they name: `route_experts`: each row names two different experts of the same group of 4 consecutive expert numbers. Among the 256 aligned rows of one index of fs, no expert is named by more than 64 rows, and in every draw some expert is named by exactly 64 rows from every such block.
All inputs are finite; a program needn't handle non-finite values.
Results may differ from a plain program's by a relative error of at most 0.018.
Values may be sent and summed in bfloat16 or wider, within the bound.
A program may use at most 64 MiB of HBM per device.

v0:
```python
import jax
import jax.numpy as jnp
from jax import lax
from jax.sharding import Mesh
from jax.sharding import PartitionSpec as P

CAP = 64
TP = ("tp_0", "tp_1")


def in_one_piece(arrays, axis, split_dim, concat_dim, along):
    ends, at = ([], 0)
    for a in arrays[:-1]:
        at += a.shape[along]
        ends.append(at)
    both = jnp.concatenate(arrays, axis=along)
    return tuple(
        jnp.split(
            lax.all_to_all(both, axis, split_axis=split_dim, concat_axis=concat_dim, tiled=True),
            ends,
            axis=along,
        )
    )


def sum_by_axis(terms, axes):
    subtotal = terms.astype(jnp.bfloat16)
    for axis in axes:
        subtotal = lax.psum_scatter(subtotal, axis, scatter_dimension=0, tiled=True)
    return subtotal.astype(jnp.float32)


def shards(
    tokens, route_experts, group_weight, pair_logit, norm_gain, gate_train, up_train, down_train
):
    experts = gate_train.shape[0]
    rows_here = gate_train.shape[1]
    model_width = norm_gain.shape[0]
    owners = lax.axis_size("fs")
    per_owner = experts // owners
    tok_rows = tokens.shape[0]
    slots_all = experts * CAP
    start_row = lax.axis_index("fs") * rows_here
    gain_rows = lax.dynamic_slice_in_dim(norm_gain, start_row, rows_here)
    gate_cast = (gain_rows[None, :, None] * gate_train).astype(jnp.bfloat16)
    up_cast = (gain_rows[None, :, None] * up_train).astype(jnp.bfloat16)
    down_cast = down_train.astype(jnp.bfloat16)
    gate_serve, up_serve, down_serve = in_one_piece((gate_cast, up_cast, down_cast), "fs", 0, 1, 2)
    expert_ids = jnp.arange(experts, dtype=jnp.int32)
    flat_hits = (route_experts.reshape(tok_rows * 2)[:, None] == expert_ids[None, :]).astype(
        jnp.int32
    )
    before = jnp.cumsum(flat_hits, axis=0) - flat_hits
    slot_index = jnp.sum(before * flat_hits, axis=1) + CAP * route_experts.reshape(tok_rows * 2)
    placed = (slot_index[:, None] == jnp.arange(slots_all, dtype=jnp.int32)[None, :]).reshape(
        tok_rows, 2, slots_all
    )
    pick_rows = (placed[:, 0] | placed[:, 1]).astype(jnp.bfloat16)
    first_gate = group_weight * jax.nn.sigmoid(pair_logit)
    second_gate = group_weight * jax.nn.sigmoid(-pair_logit)
    combine_weights = (
        placed[:, 0].astype(jnp.float32) * first_gate[:, None]
        + placed[:, 1].astype(jnp.float32) * second_gate[:, None]
    )
    contract_rows = (((0,), (0,)), ((), ()))
    outgoing = lax.dot_general(pick_rows, tokens, contract_rows, preferred_element_type=jnp.float32)
    outgoing = outgoing.astype(jnp.bfloat16).reshape(owners, per_owner, CAP, tokens.shape[1])
    arrived = lax.all_to_all(outgoing, "fs", split_axis=0, concat_axis=0, tiled=True)
    section = lax.all_gather(arrived, TP, axis=3, tiled=True)
    gate_total = jnp.einsum(
        "sexk,ekf->esxf", section, gate_serve, preferred_element_type=jnp.float32
    )
    up_total = jnp.einsum("sexk,ekf->esxf", section, up_serve, preferred_element_type=jnp.float32)
    squares_total = jnp.sum(jnp.square(section.astype(jnp.float32)), axis=3)
    row_scale = jnp.transpose(lax.rsqrt(squares_total / model_width + 1e-06), (1, 0, 2))[..., None]
    hidden = (jax.nn.silu(row_scale * gate_total) * (row_scale * up_total)).astype(jnp.bfloat16)
    summed = sum_by_axis(
        jnp.einsum("edf,esxf->dsex", down_serve, hidden, preferred_element_type=jnp.float32), TP
    )
    routed = summed.astype(jnp.bfloat16)
    returned = lax.all_to_all(routed, "fs", split_axis=1, concat_axis=1, tiled=True)
    flat_back = returned.reshape(returned.shape[0], slots_all).astype(jnp.float32)
    moe_out = lax.dot_general(
        combine_weights,
        flat_back,
        (((1,), (1,)), ((), ())),
        precision=lax.Precision.HIGHEST,
        preferred_element_type=jnp.float32,
    )
    return (gate_serve, up_serve, down_serve, moe_out.astype(jnp.bfloat16))


def solution(mesh):
    split = Mesh(
        mesh.devices.reshape(mesh.shape["grp"], mesh.shape["fs"], 8, 2),
        ("grp", "fs", "tp_0", "tp_1"),
    )
    return jax.shard_map(
        shards,
        mesh=split,
        in_specs=(
            P(("grp", "fs"), TP),
            P(("grp", "fs"), None),
            P(("grp", "fs")),
            P(("grp", "fs")),
            P(),
            P(None, "fs", TP),
            P(None, "fs", TP),
            P(None, "fs", TP),
        ),
        out_specs=(
            P(("grp", "fs"), None, TP),
            P(("grp", "fs"), None, TP),
            P(("grp", "fs"), None, TP),
            P(("grp", "fs"), TP),
        ),
        check_vma=False,
    )
```

profile of v0, /device:TPU:65, one launch (start us, length us, event | category | flops | bytes accessed | tf_op | source)
XLA Modules:
  0.0 289.9 jit_solution(10598628148280639070)
XLA Ops:
  7.3 0.9 copy.28
  8.5 1.2 reduce-window.6
  10.3 0.7 multiply_add_fusion
  11.0 0.4 iota_compare_fusion
  11.4 0.6 convolution_convert_fusion
  11.9 57.7 %all_to_all.22 = bf16[16,1,64,128]{3,2,1,0:T(8,128)(2,1)} all-to-all(bf16[16,1,64,128]{3,2,1,0:T(8,128)(2,1)S(1)} %bitcast.76), channel_id=1, replica_groups=mesh['grp'=2,'fs'=16,'tp_0'=8,'tp_1'=2] {'fs'}, dimensions={0} | all-to-all | bytes 524288 | tf_op jit(solution)/shard_map/all_to_all | solution.py:68
  69.9 0.8 dynamic_slice.3
  70.6 1.6 multiply_convert_fusion.1
  72.2 0.2 pad_maximum_fusion
  72.4 78.1 %all_to_all.23 = bf16[16,128,384]{2,1,0:T(8,128)(2,1)S(1)} all-to-all(bf16[16,128,384]{2,1,0:T(8,128)(2,1)S(1)} %pad_maximum_fusion), channel_id=1, replica_groups=mesh['grp'=2,'fs'=16,'tp_0'=8,'tp_1'=2] {'fs'}, dimensions={0} | all-to-all | bytes 3145728 | tf_op jit(solution)/shard_map/all_to_all | solution.py:19
  150.6 0.3 fusion.48
  150.9 3.6 %multiply_reduce_fusion = f32[16,64]{1,0:T(8,128)S(1)} fusion(bf16[16,1,64,2048]{3,2,0,1:T(8,128)(2,1)} %all-gather.2.cloned.1.call-done), kind=kLoop, calls=%fused_computation | loop fusion | flops 6290432 | bytes 4198400 | tf_op jit(solution)/shard_map/reduce_sum | solution.py:74
  154.6 0.3 copy-done.1
  154.9 1.2 fusion.4
  156.2 8.5 %convert_bitcast_fusion = bf16[2048,16,1,64]{0,3,1,2:T(8,128)(2,1)} fusion(bf16[16,1,64,2048]{3,2,0,1:T(8,128)(2,1)} %all-gather.2.cloned.1.call-done, bf16[1,2048,128]{2,1,0:T(8,128)(2,1)S(1)} %get-tuple-element.4, bf16[1,2048,128]{2,1,0:T(8,128)(2,1)S(1)} %get-tuple-element.5, f32[16,64,128]{2,1,0:T(8,128)S(1)} %fusion.4, f32[16,64]{1,0:T(8,128)S(1)} %add_rsqrt_fusion), kind=kOutput, calls=%fused_computation.5 | convolution fusion | flops 1076756480 | bytes 9965568 | tf_op jit(solution)/shard_map/edf,esxf->dsex/dot_general | solution.py:78
  164.8 64.4 %reduce-scatter.5.cloned.1.call-done = bf16[256,16,1,64]{0,3,1,2:T(8,128)(2,1)} async-done(((bf16[2048,16,1,64]{0,3,1,2:T(8,128)(2,1)}), bf16[256,16,1,64]{0,3,1,2:T(8,128)(2,1)}) %reduce-scatter.5.cloned.1.call-update) | async-done | bytes 524304 | tf_op jit(solution)/shard_map/reduce_scatter | solution.py:29
  229.2 2.0 copy.35
  231.2 1.5 reshape.118
  232.8 22.0 %reduce-scatter.7.cloned.1.call-done = bf16[128,1024]{1,0:T(8,128)(2,1)} async-done(((bf16[256,1024]{1,0:T(8,128)(2,1)}), bf16[128,1024]{1,0:T(8,128)(2,1)}) %reduce-scatter.7.cloned.1.call-update) | async-done | bytes 262160
  254.7 1.3 reshape.119
  256.1 1.1 copy.36
  257.2 10.7 %all-to-all-start.2 = ((bf16[128,16,1,64]{0,3,2,1:T(8,128)(2,1)}), bf16[128,16,1,64]{0,3,2,1:T(8,128)(2,1)S(1)}, u32[]{:S(2)}, u32[]{:S(2)}) async-start(bf16[128,16,1,64]{0,3,2,1:T(8,128)(2,1)} %bitcast.16), calls=%async_computation.3 | async-start | bytes 524288 | tf_op jit(solution)/shard_map/all_to_all | solution.py:81
  267.9 13.9 %all-to-all-done.2 = bf16[128,16,1,64]{0,3,2,1:T(8,128)(2,1)S(1)} async-done(((bf16[128,16,1,64]{0,3,2,1:T(8,128)(2,1)}), bf16[128,16,1,64]{0,3,2,1:T(8,128)(2,1)S(1)}, u32[]{:S(2)}, u32[]{:S(2)}) %all-to-all-start.2) | async-done | bytes 262176 | tf_op jit(solution)/shard_map/all_to_all | solution.py:81
  281.8 1.5 convolution_convert_fusion.1
  (36 shorter events, 1.4 us)
Async XLA Ops:
  7.2 4.2 %copy-start = (bf16[256,128]{1,0:T(8,128)(2,1)S(1)}, bf16[256,128]{1,0:T(8,128)(2,1)}, u32[]{:S(2)}) copy-start(bf16[256,128]{1,0:T(8,128)(2,1)} %param.8) | copy-start | bytes 196612
  7.2 62.6 %copy-start.5 = (f32[16,128,128]{2,1,0:T(8,128)S(1)}, f32[16,128,128]{2,1,0:T(8,128)}, u32[]{:S(2)}) copy-start(f32[16,128,128]{2,1,0:T(8,128)} %param.15) | copy-start | bytes 3145732
  7.2 63.4 %copy-start.6 = (f32[16,128,128]{2,1,0:T(8,128)S(1)}, f32[16,128,128]{2,1,0:T(8,128)}, u32[]{:S(2)}) copy-start(f32[16,128,128]{2,1,0:T(8,128)} %param.13) | copy-start | bytes 3145732
  7.2 143.7 %all-gather.2.cloned.1.call-start = ((), (), s32[]{:S(2)}) async-start(), calls=%async_computation.5 | async-start | bytes 4456448 | tf_op jit(solution)/shard_map/all_gather | solution.py:69
  69.7 159.5 %reduce-scatter.5.cloned.1.call-start = ((), (), s32[]{:S(2)}) async-start(), calls=%async_computation.6 | async-start | bytes 4718592 | tf_op jit(solution)/shard_map/reduce_scatter | solution.py:29
  150.8 5.3 %copy-start.4 = (bf16[1,2048,128]{2,1,0:T(8,128)(2,1)}, bf16[1,2048,128]{2,1,0:T(8,128)(2,1)S(1)}, u32[]{:S(2)}) copy-start(bf16[1,2048,128]{2,1,0:T(8,128)(2,1)S(1)} %get-tuple-element.6) | copy-start | bytes 1572868
  150.9 5.3 %copy-start.2 = (bf16[1,2048,128]{2,1,0:T(8,128)(2,1)}, bf16[1,2048,128]{2,1,0:T(8,128)(2,1)S(1)}, u32[]{:S(2)}) copy-start(bf16[1,2048,128]{2,1,0:T(8,128)(2,1)S(1)} %get-tuple-element.4) | copy-start | bytes 1572868
  150.9 5.3 %copy-start.3 = (bf16[1,2048,128]{2,1,0:T(8,128)(2,1)}, bf16[1,2048,128]{2,1,0:T(8,128)(2,1)S(1)}, u32[]{:S(2)}) copy-start(bf16[1,2048,128]{2,1,0:T(8,128)(2,1)S(1)} %get-tuple-element.5) | copy-start | bytes 1572868
  150.9 4.0 %copy-start.1 = (bf16[16,1,64,2048]{3,2,0,1:T(8,128)(2,1)S(1)}, bf16[16,1,64,2048]{3,2,0,1:T(8,128)(2,1)}, u32[]{:S(2)}) copy-start(bf16[16,1,64,2048]{3,2,0,1:T(8,128)(2,1)} %all-gather.2.cloned.1.call-done) | copy-start | bytes 12582916
  164.7 103.2 %copy-start.7 = (f32[256]{0:T(256)S(1)}, f32[256]{0:T(256)}, u32[]{:S(2)}) copy-start(f32[256]{0:T(256)} %param.10) | copy-start | bytes 3076
  164.7 103.2 %copy-start.8 = (f32[256]{0:T(256)S(1)}, f32[256]{0:T(256)}, u32[]{:S(2)}) copy-start(f32[256]{0:T(256)} %param.11) | copy-start | bytes 3076
  164.7 90.0 %reduce-scatter.7.cloned.1.call-start = ((), (), s32[]{:S(2)}) async-start(), calls=%async_computation.7 | async-start | bytes 786432
  257.2 24.6 %all-to-all-start.2 = ((bf16[128,16,1,64]{0,3,2,1:T(8,128)(2,1)}), bf16[128,16,1,64]{0,3,2,1:T(8,128)(2,1)S(1)}, u32[]{:S(2)}, u32[]{:S(2)}) async-start(bf16[128,16,1,64]{0,3,2,1:T(8,128)(2,1)} %bitcast.16), calls=%async_computation.3 | async-start | bytes 524288 | tf_op jit(solution)/shard_map/all_to_all | solution.py:81
Sparse Core Ops, SparseCore 0:
  69.8 57.9 all-gather.1
  164.9 64.2 reduce-scatter.4
  232.9 21.8 reduce-scatter.6
where the time goes:
time: 294 us; the launch traced here: 290 us
  blocking collectives  136 us (46%)
  waiting for transfers between devices  100 us (34%)
  between operations  14 us (5%)
  matrix products  11.8 us (4%)
  starting transfers between devices  10.8 us (4%)
  local copies, waits for them, and re-layouts  9.03 us (3%)
  other arithmetic  7.88 us (3%)
    all_to_all x1, blocking collectives, in_one_piece(): lax.all_to_all(both, axis, split_axis=split_dim, concat_axis=concat_dim,...  78.1 us
    reduce_scatter x1, waiting for transfers between devices, sum_by_axis(): subtotal = lax.psum_scatter(subtotal, axis, scatter_dimension=0, tiled=True)  64.4 us
    all_to_all x1, blocking collectives, shards(): lax.all_to_all(outgoing, 'fs', split_axis=0, concat_axis=0, tiled=True)  57.7 us
    unnamed x4, waiting for transfers between devices  22.1 us
    all_to_all x1, waiting for transfers between devices, shards(): lax.all_to_all(routed, 'fs', split_axis=1, concat_axis=1, tiled=True)  13.9 us
    all_to_all x1, starting transfers between devices, shards(): lax.all_to_all(routed, 'fs', split_axis=1, concat_axis=1, tiled=True)  10.7 us
    dot_general x1, matrix products, shards(): jnp.einsum('edf,esxf->dsex', down_serve, hidden, preferred_element_type=j...  8.51 us
    unnamed x23, local copies, waits for them, and re-layouts  7.27 us
  transfers between devices with their start and end apart: 4, of which 3 were waited for; matrix products, arithmetic and copies ran while one was open for 1% of the time, Pallas kernels for 0%

commit v1 on v0

v1 whole, which is shorter than its diff:
```python
import functools

import jax
import jax.numpy as jnp
from jax import lax
from jax.experimental import pallas as pl
from jax.experimental.pallas import tpu as pltpu
from jax.sharding import PartitionSpec as P

CAP = 64
MESH = pl.DeviceIdType.MESH
F32 = jnp.float32
BF16 = jnp.bfloat16
CHUNKS = 4


def ring_order(n):
    order = [n // 2]
    for far in range(n // 2 - 1, 0, -1):
        order += [far, n - far]
    return order + [0]


def dot(a, b, dims=(((1,), (0,)), ((), ()))):
    return lax.dot_general(a, b, dims, preferred_element_type=F32)


def body(
    nf,
    nx,
    pair,
    tokens,
    route,
    group_weight,
    pair_logit,
    gain,
    gate_in,
    up_in,
    down_in,
    gate_out,
    up_out,
    down_out,
    moe_out,
    stage_gu,
    stage_d,
    gain_col,
    send_tok,
    send_gu,
    send_d,
    section,
    w_gu,
    dw_own,
    dw_sib,
    h_own,
    h_sib,
    part,
    sums,
    ret,
    back,
    comb,
    sem_in,
    sem_out,
    sem_tok_s,
    sem_tok_r,
    sem_gu_s,
    sem_gu_r,
    sem_d_s,
    sem_d_r,
    sem_y_s,
    sem_y_r,
    sem_x_s,
    sem_x_r,
    sem_c_s,
    sem_c_r,
    sem_h_s,
    sem_h_r,
    sem_w_s,
    sem_w_r,
    sem_q_s,
    sem_q_r,
    sem_b_s,
    sem_b_r,
):
    g, f, t = lax.axis_index("grp"), lax.axis_index("fs"), lax.axis_index("tp")
    x, c = t // 2, t % 2
    half = g % pair
    toks = tokens.shape[0]
    rows_here = gain_col.shape[0]
    rows_half = rows_here // pair
    model = nf * rows_here
    order = ring_order(nf)
    pos = {d: p for p, d in enumerate(order)}
    per = nf // CHUNKS
    chunk_rows = per * CAP
    max_hops = nx // 2

    def hops(ch, way):
        return max_hops - (ch + way) % 2

    def zdev(d):
        return (g, (f + d) % nf, t)

    along = ((g, f, ((x + 1) % nx) * 2 + c), (g, f, ((x + nx - 1) % nx) * 2 + c))
    sib = (g, f, x * 2 + 1 - c)
    twin = (g + 1 - 2 * half, f, t)

    def rows_of(ch):
        return pl.ds(ch * chunk_rows, chunk_rows)

    def remote(src, dst, s, r, dev):
        return pltpu.make_async_remote_copy(
            src_ref=src, dst_ref=dst, send_sem=s, recv_sem=r, device_id=dev, device_id_type=MESH
        )

    def drain(ref, s):
        pltpu.make_async_copy(ref, ref, s).wait()

    mine = pl.ds(half * rows_half, rows_half)
    loads = [
        pltpu.make_async_copy(gate_in.at[:, mine], stage_gu.at[0], sem_in.at[0]),
        pltpu.make_async_copy(up_in.at[:, mine], stage_gu.at[1], sem_in.at[1]),
        pltpu.make_async_copy(down_in.at[:, mine], stage_d, sem_in.at[2]),
    ]
    for cp in loads:
        cp.start()

    barrier = pltpu.get_barrier_semaphore()
    peers = [zdev(d) for d in range(1, nf)] + [along[0], along[1], sib]
    if pair == 2:
        peers.append(twin)
    for dev in peers:
        pl.semaphore_signal(barrier, inc=1, device_id=dev, device_id_type=MESH)

    picked = route[...]
    rel = jnp.where(picked >= f, picked - f, picked - f + nf).astype(F32)
    first = jnp.broadcast_to(rel[:, 0:1], (toks, 128))
    second = jnp.broadcast_to(rel[:, 1:2], (toks, 128))
    first_t = jnp.transpose(first)[0:nf, :]
    second_t = jnp.transpose(second)[0:nf, :]
    offs = lax.broadcasted_iota(jnp.int32, (nf, toks), 0).astype(F32)
    hits_t = (first_t == offs) | (second_t == offs)
    ri = lax.broadcasted_iota(jnp.int32, (toks, toks), 0)
    ci = lax.broadcasted_iota(jnp.int32, (toks, toks), 1)
    upper = jnp.where(ri < ci, 1.0, 0.0).astype(BF16)
    rank_t = dot(jnp.where(hits_t, 1.0, 0.0).astype(BF16), upper)
    slot_t = jnp.where(hits_t, rank_t, -1.0)
    slots = lax.broadcasted_iota(jnp.int32, (CAP, toks), 0).astype(F32)
    for d in range(nf):
        pick = jnp.where(jnp.broadcast_to(slot_t[d : d + 1, :], (CAP, toks)) == slots, 1.0, 0.0)
        got = dot(pick.astype(BF16), tokens[...]).astype(BF16)
        if d == 0:
            section[t, pl.ds(pos[0] * CAP, CAP), :] = got
        else:
            send_tok[pl.ds(pos[d] * CAP, CAP), :] = got

    gain_row = gain[pl.ds(f, 1), :]
    gain_col[...] = jnp.transpose(jnp.broadcast_to(gain_row, (rows_here, rows_here)))
    scale = gain_col[mine, :]
    loads[0].wait()
    loads[1].wait()

    def cast_gu(e, carry):
        send_gu[e, :, 0:128] = (scale * stage_gu[0, e]).astype(BF16)
        send_gu[e, :, 128:256] = (scale * stage_gu[1, e]).astype(BF16)
        return carry

    lax.fori_loop(0, nf, cast_gu, 0)
    pl.semaphore_wait(barrier, len(peers))

    tok_copies = {}
    for d in reversed(order[:-1]):
        there = (nf - d) % nf
        dst = section.at[t, pl.ds(pos[there] * CAP, CAP)]
        ch = pos[there] // per
        tok_copies[d] = remote(
            send_tok.at[pl.ds(pos[d] * CAP, CAP)], dst, sem_tok_s, sem_tok_r.at[ch], zdev(d)
        )
        tok_copies[d].start()

    def w_rows(src):
        return pl.ds(pl.multiple_of(src * rows_here + half * rows_half, rows_half), rows_half)

    def d_at(src):
        return dw_own.at[(src + c) % 2, src // 2, mine]

    for d in order[:-1]:
        remote(
            send_gu.at[(f + d) % nf], w_gu.at[w_rows(f)], sem_gu_s, sem_gu_r.at[(nf - d) % nf], zdev(d)
        ).start()

    w_gu[w_rows(f), :] = send_gu[f]
    if pair == 2:
        remote(send_gu.at[f], w_gu.at[w_rows(f)], sem_y_s.at[0], sem_y_r.at[0], twin).start()

    loads[2].wait()

    def cast_d(e, carry):
        send_d[e] = stage_d[e].astype(BF16)
        return carry

    lax.fori_loop(0, nf, cast_d, 0)
    dw_own[(f + c) % 2, f // 2, mine, :] = send_d[f]

    def pass_gu(d):
        here = w_gu.at[w_rows((f + d) % nf)]
        cp = remote(here, here, sem_y_s.at[0], sem_gu_r.at[d], twin)
        cp.wait_recv()
        if pair == 2:
            remote(here, here, sem_y_s.at[0], sem_y_r.at[0], twin).start()

    def pass_d(d):
        here = d_at((f + d) % nf)
        cp = remote(here, here, sem_y_s.at[1], sem_d_r.at[d], twin)
        cp.wait_recv()
        if pair == 2:
            remote(here, here, sem_y_s.at[1], sem_y_r.at[1], twin).start()

    def gather_send(way, s, ch, blk):
        here = section.at[blk, rows_of(ch)]
        remote(here, here, sem_x_s.at[way], sem_x_r.at[way, s, ch], along[way]).start()

    def gather_share(ch, blk):
        here = section.at[blk, rows_of(ch)]
        remote(here, here, sem_c_s, sem_c_r.at[ch], sib).start()

    waiting = [d for d in order[:-1]]
    first_ch = list(reversed(range(CHUNKS)))
    for k in range(CHUNKS + max_hops):
        for i, ch in enumerate(first_ch):
            s = k - i
            if s == 0:
                count = per - (1 if pos[0] // per == ch else 0)
                drain(send_tok.at[pl.ds(0, count * CAP)], sem_tok_r.at[ch])
                for way in range(2):
                    gather_send(way, 0, ch, t)
                gather_share(ch, t)
            elif 1 <= s <= max_hops:
                for way in range(2):
                    if s > hops(ch, way):
                        continue
                    from_x = (x + (nx - s if way == 0 else s)) % nx
                    blk = from_x * 2 + c
                    here = section.at[blk, rows_of(ch)]
                    remote(
                        here, here, sem_x_s.at[way], sem_x_r.at[way, s - 1, ch], along[way]
                    ).wait_recv()
                    if s < hops(ch, way):
                        gather_send(way, s, ch, blk)
                    gather_share(ch, blk)
                if waiting:
                    pass_gu(waiting.pop(0))

    for d in order[:-1]:
        remote(
            send_d.at[(f + d) % nf], d_at(f), sem_d_s, sem_d_r.at[(nf - d) % nf], zdev(d)
        ).start()
    if pair == 2:
        remote(send_d.at[f], d_at(f), sem_y_s.at[1], sem_y_r.at[1], twin).start()
    while waiting:
        pass_gu(waiting.pop(0))

    lane = lax.broadcasted_iota(jnp.int32, (toks, 128), 1)
    lower = jnp.where(ci < ri, 1.0, 0.0).astype(BF16)
    weight = jnp.transpose(jnp.broadcast_to(group_weight[...], (128, toks)))
    logit = jnp.transpose(jnp.broadcast_to(pair_logit[...], (128, toks)))
    gate_a = weight * jax.nn.sigmoid(logit)
    gate_b = weight * jax.nn.sigmoid(-logit)
    lane_off = jnp.where(lane < CAP, 0, 1).astype(F32)
    lane_slot = jnp.where(lane < CAP, lane, lane - CAP).astype(F32)
    for k in range(nf // 2):
        off = lane_off + 2.0 * k
        is_a, is_b = first == off, second == off
        rank = dot(lower, jnp.where(is_a | is_b, 1.0, 0.0).astype(BF16))
        val = jnp.where(is_a, gate_a, 0.0) + jnp.where(is_b, gate_b, 0.0)
        val = jnp.where(rank == lane_slot, val, 0.0)
        high = val.astype(BF16)
        comb[0, :, pl.ds(k * 128, 128)] = high
        comb[1, :, pl.ds(k * 128, 128)] = (val - high.astype(F32)).astype(BF16)

    if pair == 2:
        drain(w_gu.at[pl.ds(0, nf * rows_half)], sem_y_r.at[0])
    outs = [
        pltpu.make_async_copy(w_gu.at[:, pl.ds(0, 128)], gate_out, sem_out.at[0]),
        pltpu.make_async_copy(w_gu.at[:, pl.ds(128, 128)], up_out, sem_out.at[1]),
        pltpu.make_async_copy(dw_own.at[0], down_out.at[:, c], sem_out.at[2]),
        pltpu.make_async_copy(dw_own.at[1], down_out.at[:, 1 - c], sem_out.at[3]),
    ]
    outs[0].start()
    outs[1].start()

    for ch in range(CHUNKS):
        drain(section.at[pl.ds(0, nx), pl.ds(0, chunk_rows)], sem_c_r.at[ch])
        blocks = [section[j, rows_of(ch), :] for j in range(2 * nx)]
        squares = jnp.zeros((chunk_rows, 128), F32)
        for b in blocks:
            wide = b.astype(F32)
            squares = squares + wide * wide
        row_scale = lax.rsqrt(jnp.sum(squares, axis=1, keepdims=True) / model + 1e-6)
        pre = dot(jnp.concatenate(blocks, axis=1), w_gu[...])
        gate = row_scale * pre[:, 0:128]
        up = row_scale * pre[:, 128:256]
        h_own[rows_of(ch), :] = (gate / (1.0 + jnp.exp(-gate)) * up).astype(BF16)
        remote(
            h_own.at[rows_of(ch)], h_sib.at[rows_of(ch)], sem_h_s, sem_h_r.at[ch], sib
        ).start()

    for d in order[:-1]:
        pass_d(d)
    if pair == 2:
        drain(dw_own.at[0, :, pl.ds(0, nf * rows_half // nx)], sem_y_r.at[1])
    share = remote(dw_own.at[1], dw_sib, sem_w_s, sem_w_r, sib)
    share.start()
    outs[2].start()
    outs[3].start()
    share.wait_recv()

    def sum_send(way, s, ch, src):
        remote(
            src, sums.at[way, s, rows_of(ch)], sem_q_s.at[way], sem_q_r.at[way, s, ch], along[way]
        ).start()

    def target(way, ch, s):
        left = hops(ch, way) - s
        return (x + (left if way == 0 else nx - left)) % nx

    feats = nx * 128
    for ch in range(CHUNKS):
        remote(
            h_own.at[rows_of(ch)], h_sib.at[rows_of(ch)], sem_h_s, sem_h_r.at[ch], sib
        ).wait_recv()
        both = jnp.concatenate([h_own[rows_of(ch), :], h_sib[rows_of(ch), :]], axis=1)
        down = jnp.concatenate(
            [dw_own[0].reshape(feats, 128), dw_sib[...].reshape(feats, 128)], axis=1
        )
        res = dot(both, down, (((1,), (1,)), ((), ()))).astype(BF16)
        for i in range(nx):
            part[i, rows_of(ch), :] = res[:, i * 128 : (i + 1) * 128]
        for way in range(2):
            sum_send(way, 0, ch, part.at[target(way, ch, 0), rows_of(ch)])

    for s in range(1, max_hops + 1):
        for ch in range(CHUNKS):
            for way in range(2):
                last = hops(ch, way)
                if s > last:
                    continue
                here = sums.at[way, s - 1, rows_of(ch)]
                remote(here, here, sem_q_s.at[way], sem_q_r.at[way, s - 1, ch], along[way]).wait_recv()
                if s < last:
                    sums[way, s - 1, rows_of(ch), :] = (
                        sums[way, s - 1, rows_of(ch), :].astype(F32)
                        + part[target(way, ch, s), rows_of(ch), :].astype(F32)
                    ).astype(BF16)
                    sum_send(way, s, ch, here)
            if s == max_hops:
                total = part[x, rows_of(ch), :].astype(F32)
                for way in range(2):
                    total = total + sums[way, hops(ch, way) - 1, rows_of(ch), :].astype(F32)
                ret[rows_of(ch), :] = total.astype(BF16)
                for d in order[ch * per : (ch + 1) * per]:
                    src = ret.at[pl.ds(pos[d] * CAP, CAP)]
                    if d == 0:
                        back[pl.ds(0, CAP), :] = ret[pl.ds(pos[0] * CAP, CAP), :]
                    else:
                        remote(
                            src,
                            back.at[pl.ds(((nf - d) % nf) * CAP, CAP)],
                            sem_b_s,
                            sem_b_r,
                            zdev(d),
                        ).start()

    drain(back.at[pl.ds(0, (nf - 1) * CAP)], sem_b_r)
    rows_back = back[...]
    moe_out[...] = (dot(comb[0], rows_back) + dot(comb[1], rows_back)).astype(BF16)

    for cp in outs:
        cp.wait()
    drain(send_tok.at[pl.ds(0, (nf - 1) * CAP)], sem_tok_s)
    drain(send_gu.at[pl.ds(0, nf - 1)], sem_gu_s)
    drain(send_d.at[pl.ds(0, nf - 1)], sem_d_s)
    if pair == 2:
        drain(send_gu, sem_y_s.at[0])
        drain(send_d, sem_y_s.at[1])
    for way in range(2):
        moved = sum(hops(ch, way) for ch in range(CHUNKS))
        drain(section.at[pl.ds(0, moved), pl.ds(0, chunk_rows)], sem_x_s.at[way])
        drain(section.at[pl.ds(0, moved), pl.ds(0, chunk_rows)], sem_q_s.at[way])
    drain(section.at[pl.ds(0, nx)], sem_c_s)
    drain(h_own, sem_h_s)
    share.wait_send()
    drain(ret.at[pl.ds(0, (nf - 1) * CAP)], sem_b_s)


def shards(
    nf, nt, pair, tokens, route, group_weight, pair_logit, norm_gain, gate_train, up_train, down_train
):
    nx = nt // 2
    toks, width = tokens.shape
    rows_here, units = gate_train.shape[1], gate_train.shape[2]
    rows_half = rows_here // pair
    model = norm_gain.shape[0]
    slots = nf * CAP
    max_hops = nx // 2
    vmem = pl.BlockSpec(memory_space=pltpu.VMEM)
    hbm = pl.BlockSpec(memory_space=pl.ANY)
    dma = pltpu.SemaphoreType.DMA
    gate_serve, up_serve, down_serve, moe = pl.pallas_call(
        functools.partial(body, nf, nx, pair),
        out_shape=(
            jax.ShapeDtypeStruct((model, units), BF16),
            jax.ShapeDtypeStruct((model, units), BF16),
            jax.ShapeDtypeStruct((nx, 2, rows_here, units), BF16),
            jax.ShapeDtypeStruct((toks, width), BF16),
        ),
        in_specs=[vmem] * 5 + [hbm] * 3,
        out_specs=(hbm, hbm, hbm, vmem),
        scratch_shapes=[
            pltpu.VMEM((2, nf, rows_half, units), F32),
            pltpu.VMEM((nf, rows_half, units), F32),
            pltpu.VMEM((rows_here, 128), F32),
            pltpu.VMEM((slots, width), BF16),
            pltpu.VMEM((nf, rows_half, 2 * units), BF16),
            pltpu.VMEM((nf, rows_half, units), BF16),
            pltpu.VMEM((nt, slots, width), BF16),
            pltpu.VMEM((model, 2 * units), BF16),
            pltpu.VMEM((2, nx, rows_here, units), BF16),
            pltpu.VMEM((nx, rows_here, units), BF16),
            pltpu.VMEM((slots, units), BF16),
            pltpu.VMEM((slots, units), BF16),
            pltpu.VMEM((nx, slots, width), BF16),
            pltpu.VMEM((2, max_hops, slots, width), BF16),
            pltpu.VMEM((slots, width), BF16),
            pltpu.VMEM((slots, width), BF16),
            pltpu.VMEM((2, toks, slots), BF16),
            dma((3,)),
            dma((4,)),
            dma,
            dma((CHUNKS,)),
            dma,
            dma((nf,)),
            dma,
            dma((nf,)),
            dma((2,)),
            dma((2,)),
            dma((2,)),
            dma((2, max_hops, CHUNKS)),
            dma,
            dma((CHUNKS,)),
            dma,
            dma((CHUNKS,)),
            dma,
            dma,
            dma((2,)),
            dma((2, max_hops, CHUNKS)),
            dma,
            dma,
        ],
        compiler_params=pltpu.CompilerParams(
            collective_id=0, has_side_effects=True, vmem_limit_bytes=60 * 1024 * 1024
        ),
        name="handover",
    )(
        tokens,
        route,
        group_weight.reshape(1, toks),
        pair_logit.reshape(1, toks),
        norm_gain.reshape(nf, rows_here),
        gate_train,
        up_train,
        down_train,
    )
    return (
        gate_serve.reshape(1, model, units),
        up_serve.reshape(1, model, units),
        down_serve.reshape(1, model, units),
        moe,
    )


def solution(mesh):
    nf, nt = mesh.shape["fs"], mesh.shape["tp"]
    pair = 2 if mesh.shape["grp"] % 2 == 0 else 1
    return jax.shard_map(
        functools.partial(shards, nf, nt, pair),
        mesh=mesh,
        in_specs=(
            P(("grp", "fs"), "tp"),
            P(("grp", "fs"), None),
            P(("grp", "fs")),
            P(("grp", "fs")),
            P(),
            P(None, "fs", "tp"),
            P(None, "fs", "tp"),
            P(None, "fs", "tp"),
        ),
        out_specs=(
            P(("grp", "fs"), None, "tp"),
            P(("grp", "fs"), None, "tp"),
            P(("grp", "fs"), None, "tp"),
            P(("grp", "fs"), "tp"),
        ),
        check_vma=False,
    )
```

time: 294 us -> 157 us (0.53); the launches traced: 290 us -> 157 us
  Pallas kernels: 0 us -> 150 us
  blocking collectives: 136 us -> 0 us
  waiting for transfers between devices: 100 us -> 0 us
  between operations: 14 us -> 0.66 us
  matrix products: 11.8 us -> 0 us
  starting transfers between devices: 10.8 us -> 0 us
  other arithmetic: 7.88 us -> 0 us
    pallas_call x0 -> x1, Pallas kernels: none -> 150 us  [shards(): pl.pallas_call(functools.partial(body, nf, nx, pair), out_shape=(jax.Shap...]
    all_to_all x2 -> x0, blocking collectives: 136 us -> none  [the longest x1 78.1 us: in_one_piece(): lax.all_to_all(both, axis, split_axis=split_dim, concat_axis=concat_dim,...]
    reduce_scatter x1 -> x0, waiting for transfers between devices: 64.4 us -> none  [sum_by_axis(): subtotal = lax.psum_scatter(subtotal, axis, scatter_dimension=0, tiled=True)]
    unnamed x4 -> x0, waiting for transfers between devices: 22.1 us -> none
    all_to_all x1 -> x0, waiting for transfers between devices: 13.9 us -> none  [shards(): lax.all_to_all(routed, 'fs', split_axis=1, concat_axis=1, tiled=True)]
    dot_general x4 -> x0, matrix products: 11.8 us -> none  [the longest x1 8.51 us: shards(): jnp.einsum('edf,esxf->dsex', down_serve, hidden, preferred_element_type=j...]
    all_to_all x1 -> x0, starting transfers between devices: 10.7 us -> none  [shards(): lax.all_to_all(routed, 'fs', split_axis=1, concat_axis=1, tiled=True)]
    reduce_sum x2 -> x0, other arithmetic: 3.73 us -> none  [the longest x1 3.63 us: shards(): squares_total = jnp.sum(jnp.square(section.astype(jnp.float32)), axis=3)]
  transfers between devices with their start and end apart: 4 -> 0, of which waited for: 3 -> 0; matrix products, arithmetic and copies ran while one was open for 1% -> 0% of each run, Pallas kernels for 0% -> 0%
where the time goes in v1:
time: 157 us
  Pallas kernels  150 us (96%)
  local copies, waits for them, and re-layouts  6.13 us (4%)
    pallas_call x1, Pallas kernels, shards(): pl.pallas_call(functools.partial(body, nf, nx, pair), out_shape=(jax.Shap...  150 us
    unnamed x13, local copies, waits for them, and re-layouts  6.13 us

profile of v1, /device:TPU:65, one launch (start us, length us, event | category | flops | bytes accessed | tf_op | source)
XLA Modules:
  0.0 156.8 jit_solution(15580716042713573728)
XLA Ops:
  0.6 0.0 copy-start.3
  0.6 0.7 copy-done.3
  1.3 0.8 copy.12.route
  2.1 150.0 %handover.1 = (bf16[2048,128]{1,0:T(8,128)(2,1)}, bf16[2048,128]{1,0:T(8,128)(2,1)}, bf16[8,2,128,128]{3,2,1,0:T(8,128)(2,1)}, bf16[256,128]{1,0:T(8,128)(2,1)}) custom-call(bf16[256,128]{1,0:T(8,128)(2,1)} %tokens.1, s32[256,2]{1,0:T(8,128)} %copy.12.route, f32[1,256]{1,0:T(1,128)} %bitcast.10, f32[1,256]{1,0:T(1,128)} %bitcast.11, f32[16,128]{1,0:T(8,128)} %bitcast.9, ...), custom_call_target="tpu_custom_call" | custom-call | tf_op jit(solution)/shard_map/handover/pallas_call | solution.py:408
  152.2 0.0 copy-start.1
  152.2 1.9 %copy.17 = bf16[1,2048,128]{2,1,0:T(8,128)(2,1)} copy(bf16[1,2048,128]{2,1,0:T(8,128)(2,1)} %bitcast.8) | data formatting | bytes 1048576
  154.1 0.0 copy-done.1
  154.1 0.0 copy-start
  154.1 0.8 copy.18
  154.9 0.4 copy-done
  155.3 0.0 copy-start.2
  155.3 0.8 copy.19
  156.1 0.1 copy-done.2
  156.2 0.6 copy.20
Async XLA Ops:
  0.6 0.7 copy-start.3
  152.2 1.9 %copy-start.1 = (bf16[2048,128]{1,0:T(8,128)(2,1)S(1)}, bf16[2048,128]{1,0:T(8,128)(2,1)}, u32[]{:S(2)}) copy-start(bf16[2048,128]{1,0:T(8,128)(2,1)} %get-tuple-element.9) | copy-start | bytes 1572868
  154.1 1.2 copy-start
  155.3 0.9 copy-start.2

commit v2 on v1

v2 whole, which is shorter than its diff:
```python
import functools

import jax
import jax.numpy as jnp
from jax import lax
from jax.experimental import pallas as pl
from jax.experimental.pallas import tpu as pltpu
from jax.sharding import PartitionSpec as P

CAP = 64
MESH = pl.DeviceIdType.MESH
F32 = jnp.float32
BF16 = jnp.bfloat16
CHUNKS = 4
PASS_FROM = 5
EARLY = 4
SUMS = 8
WAIT = (0, 0, 0, 0, 2, 2, 2, 2)


def ring_order(n):
    order = [n // 2]
    for far in range(n // 2 - 1, 0, -1):
        order += [far, n - far]
    return order + [0]


def dot(a, b, dims=(((1,), (0,)), ((), ()))):
    return lax.dot_general(a, b, dims, preferred_element_type=F32)


def body(
    nf,
    nx,
    pair,
    tokens_in,
    route_in,
    group_weight_in,
    pair_logit_in,
    gain_in,
    gate_in,
    up_in,
    down_in,
    gate_out,
    up_out,
    down_out,
    moe_out,
    tokens,
    route,
    group_weight,
    pair_logit,
    gain,
    stage_gu,
    stage_d,
    gain_col,
    send_tok,
    send_gu,
    send_d,
    section,
    w_gu,
    dw_own,
    dw_sib,
    h_own,
    h_sib,
    part,
    sums,
    ret,
    back,
    comb,
    ready,
    near,
    sem_in,
    sem_out,
    sem_tok_s,
    sem_tok_r,
    sem_gu_s,
    sem_gu_r,
    sem_d_s,
    sem_d_r,
    sem_y_s,
    sem_y_r,
    sem_x_s,
    sem_x_r,
    sem_c_s,
    sem_c_r,
    sem_h_s,
    sem_h_r,
    sem_w_s,
    sem_w_r,
    sem_q_s,
    sem_q_r,
    sem_b_s,
    sem_b_r,
):
    g, f, t = lax.axis_index("grp"), lax.axis_index("fs"), lax.axis_index("tp")
    x, c = t // 2, t % 2
    half = g % pair
    toks = tokens.shape[0]
    rows_here = gain_col.shape[0]
    rows_half = rows_here // pair
    model = nf * rows_here
    order = ring_order(nf)
    pos = {d: p for p, d in enumerate(order)}
    per = nf // CHUNKS
    chunk_rows = per * CAP
    max_hops = nx // 2

    def hops(ch, way):
        return max_hops - (ch + way) % 2

    def zdev(d):
        return (g, (f + d) % nf, t)

    along = ((g, f, ((x + 1) % nx) * 2 + c), (g, f, ((x + nx - 1) % nx) * 2 + c))
    sib = (g, f, x * 2 + 1 - c)
    twin = (g + 1 - 2 * half, f, t)

    def rows_of(ch):
        return pl.ds(ch * chunk_rows, chunk_rows)

    def remote(src, dst, s, r, dev):
        return pltpu.make_async_remote_copy(
            src_ref=src, dst_ref=dst, send_sem=s, recv_sem=r, device_id=dev, device_id_type=MESH
        )

    def drain(ref, s):
        pltpu.make_async_copy(ref, ref, s).wait()

    mine = pl.ds(half * rows_half, rows_half)
    small = [
        pltpu.make_async_copy(src, dst, sem_in.at[3 + i])
        for i, (src, dst) in enumerate(
            (
                (tokens_in, tokens),
                (route_in, route),
                (gain_in, gain),
                (group_weight_in, group_weight),
                (pair_logit_in, pair_logit),
            )
        )
    ]
    for cp in small:
        cp.start()
    loads = [
        pltpu.make_async_copy(gate_in.at[:, mine], stage_gu.at[0], sem_in.at[0]),
        pltpu.make_async_copy(up_in.at[:, mine], stage_gu.at[1], sem_in.at[1]),
        pltpu.make_async_copy(down_in.at[:, mine], stage_d, sem_in.at[2]),
    ]
    for cp in loads:
        cp.start()

    groups = lax.axis_size("grp")
    nt = 2 * nx
    late_first = ((groups - g) // groups) * ((nt - t) // nt)
    rank = (f + nf - late_first) % nf
    later_right = (x + 1) // nx
    earlier_left = (nx - x) // nx
    barrier = pltpu.get_barrier_semaphore()

    def greet(dev):
        pl.semaphore_signal(barrier, inc=1, device_id=dev, device_id_type=MESH)

    def tell(sem, dev):
        pl.semaphore_signal(sem, inc=1, device_id=dev, device_id_type=MESH)

    def if_later(d):
        return pl.when(rank + d < nf)

    def if_earlier(d):
        return pl.when(rank + d >= nf)

    for d in range(1, nf):
        if_later(d)(lambda d=d: greet(zdev(d)))
    pl.when(later_right == 1)(lambda: greet(along[0]))
    pl.when(earlier_left == 0)(lambda: greet(along[1]))
    pl.when(c == 1)(lambda: greet(sib))
    before = rank + (1 - later_right) + earlier_left + (1 - c)
    if pair == 2:
        pl.when(half == 1)(lambda: greet(twin))
        before = before + (1 - half)

    @pl.when(before > 0)
    def _():
        pl.semaphore_wait(barrier, before)

    for d in range(1, nf):
        if_earlier(d)(lambda d=d: tell(ready.at[nf - d], zdev(d)))
    pl.when(later_right == 0)(lambda: tell(near.at[1], along[0]))
    pl.when(earlier_left == 1)(lambda: tell(near.at[0], along[1]))
    pl.when(c == 0)(lambda: tell(near.at[2], sib))
    if pair == 2:
        pl.when(half == 0)(lambda: tell(near.at[3], twin))

    for cp in small:
        cp.wait()
    picked = route[...]
    rel = jnp.where(picked >= f, picked - f, picked - f + nf).astype(F32)
    first_t = jnp.broadcast_to(rel[0:1, :], (nf, toks))
    second_t = jnp.broadcast_to(rel[1:2, :], (nf, toks))
    offs = lax.broadcasted_iota(jnp.int32, (nf, toks), 0).astype(F32)
    hits_t = (first_t == offs) | (second_t == offs)
    ri = lax.broadcasted_iota(jnp.int32, (toks, toks), 0)
    ci = lax.broadcasted_iota(jnp.int32, (toks, toks), 1)
    upper = jnp.where(ri < ci, 1.0, 0.0).astype(BF16)
    rank_t = dot(jnp.where(hits_t, 1.0, 0.0).astype(BF16), upper)
    slot_t = jnp.where(hits_t, rank_t, -1.0)
    slots = lax.broadcasted_iota(jnp.int32, (CAP, toks), 0).astype(F32)
    for d in range(nf):
        pick = jnp.where(jnp.broadcast_to(slot_t[d : d + 1, :], (CAP, toks)) == slots, 1.0, 0.0)
        got = dot(pick.astype(BF16), tokens[...]).astype(BF16)
        if d == 0:
            section[t, pl.ds(pos[0] * CAP, CAP), :] = got
        else:
            send_tok[pl.ds(pos[d] * CAP, CAP), :] = got

    def w_rows(src):
        return pl.ds(pl.multiple_of(src * rows_here + half * rows_half, rows_half), rows_half)

    def d_at(src):
        return dw_own.at[(src + c) % 2, src // 2, mine]

    def send_rows(d):
        there = pos[(nf - d) % nf]
        remote(
            send_tok.at[pl.ds(pos[d] * CAP, CAP)],
            section.at[t, pl.ds(there * CAP, CAP)],
            sem_tok_s,
            sem_tok_r.at[there // per],
            zdev(d),
        ).start()

    def send_gate_up(d):
        remote(
            send_gu.at[(f + d) % nf], w_gu.at[w_rows(f)], sem_gu_s, sem_gu_r.at[f], zdev(d)
        ).start()

    def send_down(d):
        remote(
            send_d.at[(f + d) % nf], d_at(f), sem_d_s, sem_d_r.at[f], zdev(d)
        ).start()

    for d in order[:-1]:
        if_earlier(d)(lambda d=d: send_rows(d))

    gain_row = gain[pl.ds(f, 1), :]
    gain_col[...] = jnp.transpose(jnp.broadcast_to(gain_row, (rows_here, rows_here)))
    scale = gain_col[mine, :]
    loads[0].wait()
    loads[1].wait()

    def cast_gu(e, carry):
        send_gu[e, :, 0:128] = (scale * stage_gu[0, e]).astype(BF16)
        send_gu[e, :, 128:256] = (scale * stage_gu[1, e]).astype(BF16)
        return carry

    lax.fori_loop(0, nf, cast_gu, 0)
    w_gu[w_rows(f), :] = send_gu[f]
    loads[2].wait()

    def cast_d(e, carry):
        send_d[e] = stage_d[e].astype(BF16)
        return carry

    lax.fori_loop(0, nf, cast_d, 0)
    dw_own[(f + c) % 2, f // 2, mine, :] = send_d[f]

    first_in = nf // 2 + EARLY

    def send_weights(d):
        send_gate_up(d)
        send_down(d)

    def if_early(d):
        return pl.when((rank < first_in) & ((rank + d < first_in) | (rank + d >= nf)))

    def late(d):
        return (rank >= first_in) | ((rank + d < nf) & (rank + d >= first_in))

    def if_late(d):
        return pl.when(late(d))

    for d in order[:-1]:
        pl.when((rank + d >= nf) & (rank < first_in))(lambda d=d: send_weights(d))
    for d in range(1, nf):

        @if_later(d)
        def _(d=d):
            pl.semaphore_wait(ready.at[d], 1)
            send_rows(d)

        pl.when(rank + d < first_in)(lambda d=d: send_weights(d))

    def burst(guard):
        for step in (send_gate_up, send_down):
            for d in order[:-1]:
                pl.when(guard(d))(lambda d=d, step=step: step(d))

    burst(lambda d: rank == nf - 1)

    @pl.when(later_right == 1)
    def _():
        pl.semaphore_wait(near.at[0], 1)

    @pl.when(earlier_left == 0)
    def _():
        pl.semaphore_wait(near.at[1], 1)

    @pl.when(c == 1)
    def _():
        pl.semaphore_wait(near.at[2], 1)

    if pair == 2:

        @pl.when(half == 1)
        def _():
            pl.semaphore_wait(near.at[3], 1)

        remote(send_gu.at[f], w_gu.at[w_rows(f)], sem_y_s.at[0], sem_y_r.at[0], twin).start()
        remote(send_d.at[f], d_at(f), sem_y_s.at[1], sem_y_r.at[1], twin).start()

    def pass_gu(d):
        src = (f + d) % nf
        here = w_gu.at[w_rows(src)]
        remote(here, here, sem_y_s.at[0], sem_gu_r.at[src], twin).wait_recv()
        if pair == 2:
            remote(here, here, sem_y_s.at[0], sem_y_r.at[0], twin).start()

    def pass_d(d):
        src = (f + d) % nf
        here = d_at(src)
        remote(here, here, sem_y_s.at[1], sem_d_r.at[src], twin).wait_recv()
        if pair == 2:
            remote(here, here, sem_y_s.at[1], sem_y_r.at[1], twin).start()

    def gather_send(way, s, ch, blk):
        here = section.at[blk, rows_of(ch)]
        remote(here, here, sem_x_s.at[way], sem_x_r.at[way, s, ch], along[way]).start()

    def gather_share(ch, blk):
        here = section.at[blk, rows_of(ch)]
        remote(here, here, sem_c_s, sem_c_r.at[ch], sib).start()

    def gather_own(ch):
        count = per - (1 if pos[0] // per == ch else 0)
        drain(send_tok.at[pl.ds(0, count * CAP)], sem_tok_r.at[ch])
        for way in range(2):
            gather_send(way, 0, ch, t)
        gather_share(ch, t)

    def gather_step(s, ch):
        for way in range(2):
            if s > hops(ch, way):
                continue
            from_x = (x + (nx - s if way == 0 else s)) % nx
            blk = from_x * 2 + c
            here = section.at[blk, rows_of(ch)]
            remote(
                here, here, sem_x_s.at[way], sem_x_r.at[way, s - 1, ch], along[way]
            ).wait_recv()
            if s < hops(ch, way):
                gather_send(way, s, ch, blk)
            gather_share(ch, blk)

    def hidden(ch):
        drain(section.at[pl.ds(0, nx), pl.ds(0, chunk_rows)], sem_c_r.at[ch])
        blocks = [section[j, rows_of(ch), :] for j in range(2 * nx)]
        squares = jnp.zeros((chunk_rows, 128), F32)
        for b in blocks:
            wide = b.astype(F32)
            squares = squares + wide * wide
        row_scale = lax.rsqrt(jnp.sum(squares, axis=1, keepdims=True) / model + 1e-6)
        pre = dot(jnp.concatenate(blocks, axis=1), w_gu[...])
        gate = row_scale * pre[:, 0:128]
        up = row_scale * pre[:, 128:256]
        h_own[rows_of(ch), :] = (gate / (1.0 + jnp.exp(-gate)) * up).astype(BF16)
        remote(
            h_own.at[rows_of(ch)], h_sib.at[rows_of(ch)], sem_h_s, sem_h_r.at[ch], sib
        ).start()

    sum_rows = nf * CAP // SUMS
    per_sum = nf // SUMS

    def srows(u):
        return pl.ds(u * sum_rows, sum_rows)

    def sum_send(way, s, u, src):
        remote(
            src, sums.at[way, s, srows(u)], sem_q_s.at[way], sem_q_r.at[way, s, u], along[way]
        ).start()

    def target(way, u, s):
        left = hops(u, way) - s
        return (x + (left if way == 0 else nx - left)) % nx

    feats = nx * 128

    def partials(ch):
        remote(
            h_own.at[rows_of(ch)], h_sib.at[rows_of(ch)], sem_h_s, sem_h_r.at[ch], sib
        ).wait_recv()
        both = jnp.concatenate([h_own[rows_of(ch), :], h_sib[rows_of(ch), :]], axis=1)
        down = jnp.concatenate(
            [dw_own[0].reshape(feats, 128), dw_sib[...].reshape(feats, 128)], axis=1
        )
        res = dot(both, down, (((1,), (1,)), ((), ()))).astype(BF16)
        for i in range(nx):
            part[i, rows_of(ch), :] = res[:, i * 128 : (i + 1) * 128]

    def sum_step(s, u):
        for way in range(2):
            last = hops(u, way)
            if s > last:
                continue
            if s == 0:
                sum_send(way, 0, u, part.at[target(way, u, 0), srows(u)])
                continue
            here = sums.at[way, s - 1, srows(u)]
            remote(here, here, sem_q_s.at[way], sem_q_r.at[way, s - 1, u], along[way]).wait_recv()
            if s < last:
                sums[way, s - 1, srows(u), :] = (
                    sums[way, s - 1, srows(u), :].astype(F32)
                    + part[target(way, u, s), srows(u), :].astype(F32)
                ).astype(BF16)
                sum_send(way, s, u, here)
        if s < max_hops:
            return
        total = part[x, srows(u), :].astype(F32)
        for way in range(2):
            total = total + sums[way, hops(u, way) - 1, srows(u), :].astype(F32)
        ret[srows(u), :] = total.astype(BF16)
        for d in order[u * per_sum : (u + 1) * per_sum]:
            if d == 0:
                back[pl.ds(0, CAP), :] = ret[pl.ds(pos[0] * CAP, CAP), :]
            else:
                remote(
                    ret.at[pl.ds(pos[d] * CAP, CAP)],
                    back.at[pl.ds(((nf - d) % nf) * CAP, CAP)],
                    sem_b_s,
                    sem_b_r,
                    zdev(d),
                ).start()

    for ch in reversed(range(CHUNKS)):
        gather_own(ch)

    burst(lambda d: (rank < nf - 1) & late(d))
    for step in (pass_gu, pass_d):
        for d in order[:-1]:
            if_early(d)(lambda d=d, step=step: step(d))
    waiting = [(step, d) for step in (pass_gu, pass_d) for d in order[:-1]]
    event = 0
    for s in range(1, max_hops + 1):
        for ch in reversed(range(CHUNKS)):
            gather_step(s, ch)
            event += 1
            if event > PASS_FROM:
                for step, d in (waiting.pop(0), waiting.pop(0)):
                    if_late(d)(functools.partial(step, d))
    outs = [
        pltpu.make_async_copy(w_gu.at[:, pl.ds(0, 128)], gate_out, sem_out.at[0]),
        pltpu.make_async_copy(w_gu.at[:, pl.ds(128, 128)], up_out, sem_out.at[1]),
        pltpu.make_async_copy(dw_own.at[0], down_out.at[:, c], sem_out.at[2]),
        pltpu.make_async_copy(dw_own.at[1], down_out.at[:, 1 - c], sem_out.at[3]),
    ]
    while waiting and waiting[0][0] is pass_gu:
        step, d = waiting.pop(0)
        if_late(d)(lambda: step(d))
    if pair == 2:
        drain(w_gu.at[pl.ds(0, nf * rows_half)], sem_y_r.at[0])
    outs[0].start()
    outs[1].start()
    for ch in range(CHUNKS):
        hidden(ch)
    for step, d in waiting:
        if_late(d)(lambda: step(d))
    if pair == 2:
        drain(dw_own.at[0, :, pl.ds(0, nf * rows_half // nx)], sem_y_r.at[1])
    share = remote(dw_own.at[1], dw_sib, sem_w_s, sem_w_r, sib)
    share.start()
    outs[2].start()
    outs[3].start()
    share.wait_recv()
    for ch in range(CHUNKS):
        partials(ch)
        for u in range(ch * SUMS // CHUNKS, (ch + 1) * SUMS // CHUNKS):
            if WAIT[u] == 0:
                sum_step(0, u)

    lane = lax.broadcasted_iota(jnp.int32, (toks, 128), 1)
    lower = jnp.where(ci < ri, 1.0, 0.0).astype(BF16)
    first = jnp.transpose(jnp.broadcast_to(rel[0:1, :], (128, toks)))
    second = jnp.transpose(jnp.broadcast_to(rel[1:2, :], (128, toks)))
    weight = jnp.transpose(jnp.broadcast_to(group_weight[...], (128, toks)))
    logit = jnp.transpose(jnp.broadcast_to(pair_logit[...], (128, toks)))
    gate_a = weight * jax.nn.sigmoid(logit)
    gate_b = weight * jax.nn.sigmoid(-logit)
    lane_off = jnp.where(lane < CAP, 0, 1).astype(F32)
    lane_slot = jnp.where(lane < CAP, lane, lane - CAP).astype(F32)
    for k in range(nf // 2):
        off = lane_off + 2.0 * k
        is_a, is_b = first == off, second == off
        seen = dot(lower, jnp.where(is_a | is_b, 1.0, 0.0).astype(BF16))
        val = jnp.where(is_a, gate_a, 0.0) + jnp.where(is_b, gate_b, 0.0)
        val = jnp.where(seen == lane_slot, val, 0.0)
        high = val.astype(BF16)
        comb[0, :, pl.ds(k * 128, 128)] = high
        comb[1, :, pl.ds(k * 128, 128)] = (val - high.astype(F32)).astype(BF16)

    for k in range(1, max_hops + 1 + max(WAIT)):
        for u in range(SUMS):
            s = k - WAIT[u]
            if 0 <= s <= max_hops:
                sum_step(s, u)

    drain(back.at[pl.ds(0, (nf - 1) * CAP)], sem_b_r)
    rows_back = back[...]
    moe_out[...] = (dot(comb[0], rows_back) + dot(comb[1], rows_back)).astype(BF16)

    for cp in outs:
        cp.wait()
    drain(send_tok.at[pl.ds(0, (nf - 1) * CAP)], sem_tok_s)
    drain(send_gu.at[pl.ds(0, nf - 1)], sem_gu_s)
    drain(send_d.at[pl.ds(0, nf - 1)], sem_d_s)
    if pair == 2:
        drain(send_gu, sem_y_s.at[0])
        drain(send_d, sem_y_s.at[1])
    for way in range(2):
        moved = sum(hops(ch, way) for ch in range(CHUNKS))
        drain(section.at[pl.ds(0, moved), pl.ds(0, chunk_rows)], sem_x_s.at[way])
        moved = sum(hops(u, way) for u in range(SUMS))
        drain(section.at[pl.ds(0, nx // 2), pl.ds(0, moved * sum_rows // (nx // 2))], sem_q_s.at[way])
    drain(section.at[pl.ds(0, nx)], sem_c_s)
    drain(h_own, sem_h_s)
    share.wait_send()
    drain(ret.at[pl.ds(0, (nf - 1) * CAP)], sem_b_s)


def shards(
    nf, nt, pair, tokens, route, group_weight, pair_logit, norm_gain, gate_train, up_train, down_train
):
    nx = nt // 2
    toks, width = tokens.shape
    rows_here, units = gate_train.shape[1], gate_train.shape[2]
    rows_half = rows_here // pair
    model = norm_gain.shape[0]
    slots = nf * CAP
    max_hops = nx // 2
    vmem = pl.BlockSpec(memory_space=pltpu.VMEM)
    hbm = pl.BlockSpec(memory_space=pl.ANY)
    dma = pltpu.SemaphoreType.DMA
    gate_serve, up_serve, down_serve, moe = pl.pallas_call(
        functools.partial(body, nf, nx, pair),
        out_shape=(
            jax.ShapeDtypeStruct((model, units), BF16),
            jax.ShapeDtypeStruct((model, units), BF16),
            jax.ShapeDtypeStruct((nx, 2, rows_here, units), BF16),
            jax.ShapeDtypeStruct((toks, width), BF16),
        ),
        in_specs=[hbm] * 8,
        out_specs=(hbm, hbm, hbm, vmem),
        scratch_shapes=[
            pltpu.VMEM((toks, width), BF16),
            pltpu.VMEM((2, toks), jnp.int32),
            pltpu.VMEM((1, toks), F32),
            pltpu.VMEM((1, toks), F32),
            pltpu.VMEM((nf, rows_here), F32),
            pltpu.VMEM((2, nf, rows_half, units), F32),
            pltpu.VMEM((nf, rows_half, units), F32),
            pltpu.VMEM((rows_here, 128), F32),
            pltpu.VMEM((slots, width), BF16),
            pltpu.VMEM((nf, rows_half, 2 * units), BF16),
            pltpu.VMEM((nf, rows_half, units), BF16),
            pltpu.VMEM((nt, slots, width), BF16),
            pltpu.VMEM((model, 2 * units), BF16),
            pltpu.VMEM((2, nx, rows_here, units), BF16),
            pltpu.VMEM((nx, rows_here, units), BF16),
            pltpu.VMEM((slots, units), BF16),
            pltpu.VMEM((slots, units), BF16),
            pltpu.VMEM((nx, slots, width), BF16),
            pltpu.VMEM((2, max_hops, slots, width), BF16),
            pltpu.VMEM((slots, width), BF16),
            pltpu.VMEM((slots, width), BF16),
            pltpu.VMEM((2, toks, slots), BF16),
            pltpu.SemaphoreType.REGULAR((nf,)),
            pltpu.SemaphoreType.REGULAR((4,)),
            dma((8,)),
            dma((4,)),
            dma,
            dma((CHUNKS,)),
            dma,
            dma((nf,)),
            dma,
            dma((nf,)),
            dma((2,)),
            dma((2,)),
            dma((2,)),
            dma((2, max_hops, CHUNKS)),
            dma,
            dma((CHUNKS,)),
            dma,
            dma((CHUNKS,)),
            dma,
            dma,
            dma((2,)),
            dma((2, max_hops, SUMS)),
            dma,
            dma,
        ],
        compiler_params=pltpu.CompilerParams(
            collective_id=0, has_side_effects=True, vmem_limit_bytes=60 * 1024 * 1024
        ),
        name="handover",
    )(
        tokens,
        route.T,
        group_weight.reshape(1, toks),
        pair_logit.reshape(1, toks),
        norm_gain.reshape(nf, rows_here),
        gate_train,
        up_train,
        down_train,
    )
    return (
        gate_serve.reshape(1, model, units),
        up_serve.reshape(1, model, units),
        down_serve.reshape(1, model, units),
        moe,
    )


def solution(mesh):
    nf, nt = mesh.shape["fs"], mesh.shape["tp"]
    pair = 2 if mesh.shape["grp"] % 2 == 0 else 1
    return jax.shard_map(
        functools.partial(shards, nf, nt, pair),
        mesh=mesh,
        in_specs=(
            P(("grp", "fs"), "tp"),
            P(("grp", "fs"), None),
            P(("grp", "fs")),
            P(("grp", "fs")),
            P(),
            P(None, "fs", "tp"),
            P(None, "fs", "tp"),
            P(None, "fs", "tp"),
        ),
        out_specs=(
            P(("grp", "fs"), None, "tp"),
            P(("grp", "fs"), None, "tp"),
            P(("grp", "fs"), None, "tp"),
            P(("grp", "fs"), "tp"),
        ),
        check_vma=False,
    )
```

time: 157 us -> 147 us (0.936)
  Pallas kernels: 150 us -> 141 us
    pallas_call x1, Pallas kernels: 150 us -> 141 us  [shards(): pl.pallas_call(functools.partial(body, nf, nx, pair), out_shape=(jax.Shap...]
    unnamed x13 -> x10, local copies, waits for them, and re-layouts: 6.13 us -> 4.65 us
where the time goes in v2:
time: 147 us; the launch traced here: 146 us
  Pallas kernels  141 us (96%)
  local copies, waits for them, and re-layouts  4.65 us (3%)
    pallas_call x1, Pallas kernels, shards(): pl.pallas_call(functools.partial(body, nf, nx, pair), out_shape=(jax.Shap...  141 us
    unnamed x10, local copies, waits for them, and re-layouts  4.65 us

profile of v2, /device:TPU:65, one launch (start us, length us, event | category | flops | bytes accessed | tf_op | source)
XLA Modules:
  0.0 146.2 jit_solution(3617908834414203915)
XLA Ops:
  0.6 140.9 %handover.1 = (bf16[2048,128]{1,0:T(8,128)(2,1)}, bf16[2048,128]{1,0:T(8,128)(2,1)}, bf16[8,2,128,128]{3,2,1,0:T(8,128)(2,1)}, bf16[256,128]{1,0:T(8,128)(2,1)}) custom-call(bf16[256,128]{1,0:T(8,128)(2,1)} %tokens_in.1, s32[2,256]{1,0:T(2,128)} %bitcast.11, f32[1,256]{1,0:T(1,128)} %bitcast.12, f32[1,256]{1,0:T(1,128)} %bitcast.13, f32[16,128]{1,0:T(8,128)} %bitcast.10, ...), custom_call_target="tpu_custom_call" | custom-call | tf_op jit(solution)/shard_map/handover/pallas_call | solution.py:551
  141.5 0.0 copy-start.1
  141.5 1.9 %copy.16 = bf16[1,2048,128]{2,1,0:T(8,128)(2,1)} copy(bf16[1,2048,128]{2,1,0:T(8,128)(2,1)} %bitcast.9) | data formatting | bytes 1048576
  143.4 0.0 copy-done.1
  143.5 0.0 copy-start
  143.5 0.8 copy.17
  144.2 0.4 copy-done
  144.7 0.0 copy-start.2
  144.7 0.8 copy.18
  145.5 0.1 copy-done.2
  145.5 0.6 copy.19
Async XLA Ops:
  141.5 1.9 %copy-start.1 = (bf16[2048,128]{1,0:T(8,128)(2,1)S(1)}, bf16[2048,128]{1,0:T(8,128)(2,1)}, u32[]{:S(2)}) copy-start(bf16[2048,128]{1,0:T(8,128)(2,1)} %get-tuple-element.9) | copy-start | bytes 1572868
  143.5 1.2 copy-start
  144.7 0.9 copy-start.2

commit v3 on v2

--- a/solution.py
+++ b/solution.py
@@ -462,17 +462,14 @@
         pltpu.make_async_copy(dw_own.at[0], down_out.at[:, c], sem_out.at[2]),
         pltpu.make_async_copy(dw_own.at[1], down_out.at[:, 1 - c], sem_out.at[3]),
     ]
-    while waiting and waiting[0][0] is pass_gu:
-        step, d = waiting.pop(0)
-        if_late(d)(lambda: step(d))
+    for step, d in waiting:
+        if_late(d)(functools.partial(step, d))
     if pair == 2:
         drain(w_gu.at[pl.ds(0, nf * rows_half)], sem_y_r.at[0])
     outs[0].start()
     outs[1].start()
     for ch in range(CHUNKS):
         hidden(ch)
-    for step, d in waiting:
-        if_late(d)(lambda: step(d))
     if pair == 2:
         drain(dw_own.at[0, :, pl.ds(0, nf * rows_half // nx)], sem_y_r.at[1])
     share = remote(dw_own.at[1], dw_sib, sem_w_s, sem_w_r, sib)
@@ -533,6 +530,27 @@
     drain(h_own, sem_h_s)
     share.wait_send()
     drain(ret.at[pl.ds(0, (nf - 1) * CAP)], sem_b_s)
+
+
+def deliver(*refs):
+    n = len(refs) // 3
+    sources, outs, held = refs[:n], refs[n : 2 * n], refs[2 * n : 3 * n]
+    sem_in, sem_out = refs[3 * n :]
+    takes, gives = [], []
+    for i in range(n):
+        rows = sources[i].shape[0] // 2
+        for part in range(2):
+            at = pl.ds(part * rows, rows)
+            k = 2 * i + part
+            takes.append(pltpu.make_async_copy(sources[i].at[at], held[i].at[at], sem_in.at[k]))
+            gives.append(pltpu.make_async_copy(held[i].at[at], outs[i].at[at], sem_out.at[k]))
+    for cp in takes:
+        cp.start()
+    for take, give in zip(takes, gives):
+        take.wait()
+        give.start()
+    for cp in gives:
+        cp.wait()
 
 
 def shards(
@@ -620,6 +638,17 @@
         up_train,
         down_train,
     )
+    made = (gate_serve, up_serve, down_serve, moe)
+    gate_serve, up_serve, down_serve, moe = pl.pallas_call(
+        deliver,
+        out_shape=tuple(jax.ShapeDtypeStruct(a.shape, a.dtype) for a in made),
+        in_specs=[hbm] * len(made),
+        out_specs=(hbm,) * len(made),
+        scratch_shapes=[pltpu.VMEM(a.shape, a.dtype) for a in made]
+        + [dma((2 * len(made),)), dma((2 * len(made),))],
+        compiler_params=pltpu.CompilerParams(vmem_limit_bytes=60 * 1024 * 1024),
+        name="deliver",
+    )(*made)
     return (
         gate_serve.reshape(1, model, units),
         up_serve.reshape(1, model, units),

time: 147 us -> 142 us (0.966)
  local copies, waits for them, and re-layouts: 4.65 us -> 0 us
    unnamed x10 -> x0, local copies, waits for them, and re-layouts: 4.65 us -> none
    pallas_call x1, Pallas kernels: 141 us -> 139 us  [shards(): pl.pallas_call(functools.partial(body, nf, nx, pair), out_shape=(jax.Shap...]
    pallas_call x0 -> x1, Pallas kernels: none -> 2.23 us  [shards(): pl.pallas_call(deliver, out_shape=tuple((jax.ShapeDtypeStruct(a.shape, a....]
where the time goes in v3:
time: 142 us
  Pallas kernels  141 us (99%)
    pallas_call x1, Pallas kernels, shards(): pl.pallas_call(functools.partial(body, nf, nx, pair), out_shape=(jax.Shap...  139 us

profile of v3, /device:TPU:65, one launch (start us, length us, event | category | flops | bytes accessed | tf_op | source)
XLA Modules:
  0.0 141.6 jit_solution(706345022856285753)
XLA Ops:
  0.6 138.5 %handover.1 = (bf16[2048,128]{1,0:T(8,128)(2,1)}, bf16[2048,128]{1,0:T(8,128)(2,1)}, bf16[8,2,128,128]{3,2,1,0:T(8,128)(2,1)}, bf16[256,128]{1,0:T(8,128)(2,1)}) custom-call(bf16[256,128]{1,0:T(8,128)(2,1)} %tokens_in.1, s32[2,256]{1,0:T(2,128)} %bitcast.8, f32[1,256]{1,0:T(1,128)} %bitcast.9, f32[1,256]{1,0:T(1,128)} %bitcast.10, f32[16,128]{1,0:T(8,128)} %bitcast.7, ...), custom_call_target="tpu_custom_call" | custom-call | tf_op jit(solution)/shard_map/handover/pallas_call | solution.py:569
  139.2 2.2 %deliver.1 = (bf16[2048,128]{1,0:T(8,128)(2,1)}, bf16[2048,128]{1,0:T(8,128)(2,1)}, bf16[8,2,128,128]{3,2,1,0:T(8,128)(2,1)}, bf16[256,128]{1,0:T(8,128)(2,1)}) custom-call(bf16[2048,128]{1,0:T(8,128)(2,1)} %get-tuple-element.12.refs_0_, bf16[2048,128]{1,0:T(8,128)(2,1)} %get-tuple-element.13.refs_1_, bf16[8,2,128,128]{3,2,1,0:T(8,128)(2,1)} %get-tuple-element.14.refs_2_, ...), custom_call_target="tpu_custom_call" | custom-call | tf_op jit(solution)/shard_map/deliver/pallas_call | solution.py:642

commit v4 on v3

--- a/solution.py
+++ b/solution.py
@@ -12,7 +12,7 @@
 F32 = jnp.float32
 BF16 = jnp.bfloat16
 CHUNKS = 4
-PASS_FROM = 5
+PASS_FROM = 8
 EARLY = 4
 SUMS = 8
 WAIT = (0, 0, 0, 0, 2, 2, 2, 2)

time: 142 us -> 143 us (level)
  no operation moved by 1% of the time
where the time goes in v4:
time: 143 us; the launch traced here: 142 us
  Pallas kernels  141 us (99%)
    pallas_call x1, Pallas kernels, shards(): pl.pallas_call(functools.partial(body, nf, nx, pair), out_shape=(jax.Shap...  139 us

profile of v4, /device:TPU:65, one launch (start us, length us, event | category | flops | bytes accessed | tf_op | source)
XLA Modules:
  0.0 142.3 jit_solution(1883052521871709165)
XLA Ops:
  0.6 139.2 %handover.1 = (bf16[2048,128]{1,0:T(8,128)(2,1)}, bf16[2048,128]{1,0:T(8,128)(2,1)}, bf16[8,2,128,128]{3,2,1,0:T(8,128)(2,1)}, bf16[256,128]{1,0:T(8,128)(2,1)}) custom-call(bf16[256,128]{1,0:T(8,128)(2,1)} %tokens_in.1, s32[2,256]{1,0:T(2,128)} %bitcast.8, f32[1,256]{1,0:T(1,128)} %bitcast.9, f32[1,256]{1,0:T(1,128)} %bitcast.10, f32[16,128]{1,0:T(8,128)} %bitcast.7, ...), custom_call_target="tpu_custom_call" | custom-call | tf_op jit(solution)/shard_map/handover/pallas_call | solution.py:569
  139.9 2.2 %deliver.1 = (bf16[2048,128]{1,0:T(8,128)(2,1)}, bf16[2048,128]{1,0:T(8,128)(2,1)}, bf16[8,2,128,128]{3,2,1,0:T(8,128)(2,1)}, bf16[256,128]{1,0:T(8,128)(2,1)}) custom-call(bf16[2048,128]{1,0:T(8,128)(2,1)} %get-tuple-element.12.refs_0_, bf16[2048,128]{1,0:T(8,128)(2,1)} %get-tuple-element.13.refs_1_, bf16[8,2,128,128]{3,2,1,0:T(8,128)(2,1)} %get-tuple-element.14.refs_2_, ...), custom_call_target="tpu_custom_call" | custom-call | tf_op jit(solution)/shard_map/deliver/pallas_call | solution.py:642
